TPU v7x, 32 devices: a whole 2x2x4 slice. The times are simulated.
32 devices in a mesh: sp: 16 (over z, y, core), tp: 2 (over x).
Axes of the slice: x: 2, y: 2, z: 4, core: 2. Of those that a mesh axis runs over, the one named last changes fastest.
Arguments:
- query_rows: bfloat16 [8192, 1024], P(('sp', 'tp')), may hold values from -6 to 6
- key_rows: bfloat16 [8192, 1024], P(('sp', 'tp')), may hold values from -6 to 6
- value_rows: bfloat16 [8192, 1024], P(('sp', 'tp')), may hold values from -6 to 6
- out_grad: bfloat16 [8192, 1024], P(('sp', 'tp')), may hold values from -40 to 40
- log_totals: float32 [8192, 8], P(('sp', 'tp')), may hold values from 6 to 7.5
- out_dot: float32 [8192, 8], P(('sp', 'tp')), may hold values from -6 to 6
- bias_table: float32 [8, 320], replicated, may hold values from -4 to 4
Outputs:
- grad_query: bfloat16 [8192, 1024], P(('sp', 'tp'))
- grad_key: bfloat16 [8192, 1024], P(('sp', 'tp'))
- grad_value: bfloat16 [8192, 1024], P(('sp', 'tp'))
- grad_table: float32 [8, 320], replicated
All inputs are finite; a program needn't handle non-finite values.
Results may differ from a plain program's by a relative error of at most 0.005.
Values may be sent and summed in bfloat16 or wider, within the bound.
No kernel may reach another device: no remote copies, remote signals or barrier semaphores. Data moves between devices by JAX's collectives and lax.ppermute only.
A program may use at most 128 MiB of HBM per device.

v0:
```python
import jax
import jax.numpy as jnp
from jax import lax
from jax.sharding import PartitionSpec as P

SEG_LEN = 64
LEFT_SEGS = 8
REL_CLIP = 256


def passed_along(block, axis, distance):
    devices = range(lax.axis_size(axis))
    route = [(i - distance, i) for i in devices if i - distance in devices]
    return lax.ppermute(block, axis, route)


def band_matrix(diagonal_vals, row_count, col_count):
    head_count = diagonal_vals.shape[0]
    span_width = row_count + col_count - 1
    repeated = jnp.broadcast_to(diagonal_vals[:, None, :], (head_count, row_count, span_width))
    flat_rows = jnp.pad(
        repeated.reshape(head_count, row_count * span_width), ((0, 0), (0, row_count))
    )
    shaped = flat_rows.reshape(head_count, row_count, span_width + 1)[:, :, :col_count]
    return shaped[:, :, ::-1]


def diagonal_sums(matrix_vals):
    head_count, row_count, col_count = matrix_vals.shape
    span_width = row_count + col_count - 1
    flipped = jnp.pad(matrix_vals[:, :, ::-1], ((0, 0), (0, 0), (0, row_count)))
    skewed = flipped.reshape(head_count, row_count * (col_count + row_count))[
        :, : row_count * span_width
    ]
    return jnp.sum(skewed.reshape(head_count, row_count, span_width), axis=1)


def table_onehot(offset, row_count, col_count, table_len):
    diagonals = jnp.arange(row_count + col_count - 1, dtype=jnp.int32)
    distance = jnp.clip(offset + diagonals - (col_count - 1), 1 - SEG_LEN, REL_CLIP) + SEG_LEN - 1
    return (distance[:, None] == jnp.arange(table_len, dtype=jnp.int32)[None, :]).astype(
        jnp.float32
    )


def bias_block(bias_table, offset, row_count, col_count):
    onehot_map = table_onehot(offset, row_count, col_count, bias_table.shape[1])
    diagonal_vals = jnp.dot(bias_table, onehot_map.T, precision=lax.Precision.HIGHEST)
    return (band_matrix(diagonal_vals, row_count, col_count), onehot_map)


def band_stack(rows, block_count, span_segs):
    segmented = rows.reshape(-1, SEG_LEN, rows.shape[1])
    pieces = [segmented[start : start + block_count] for start in range(span_segs)]
    return jnp.stack(pieces, axis=1).reshape(block_count, span_segs * SEG_LEN, rows.shape[1])


def band_terms(queries, grads_out, log_rows, dot_rows, keys, values, bias_vals, allowed):
    block_count, query_count, feature_count = queries.shape
    key_count = keys.shape[1]
    head_count = log_rows.shape[2]
    query_heads = queries.reshape(block_count, query_count, head_count, -1)
    grad_heads = grads_out.reshape(block_count, query_count, head_count, -1)
    key_heads = keys.reshape(block_count, key_count, head_count, -1)
    value_heads = values.reshape(block_count, key_count, head_count, -1)
    inv_root = query_heads.shape[3] ** (-0.5)
    raw_scores = jnp.einsum(
        "bqhd,bkhd->bhqk", query_heads, key_heads, preferred_element_type=jnp.float32
    )
    scores = raw_scores * inv_root + bias_vals[None]
    log_terms = jnp.transpose(log_rows, (0, 2, 1))[:, :, :, None]
    dot_terms = jnp.transpose(dot_rows, (0, 2, 1))[:, :, :, None]
    weights = jnp.exp(scores - log_terms)
    weights = jnp.where(allowed[:, None, None, :], weights, 0.0)
    weight_grads = jnp.einsum(
        "bqhd,bkhd->bhqk", grad_heads, value_heads, preferred_element_type=jnp.float32
    )
    score_grads = weights * (weight_grads - dot_terms)
    return (
        weights.astype(jnp.bfloat16),
        score_grads.astype(jnp.bfloat16),
        score_grads,
        query_heads,
        key_heads,
        grad_heads,
        inv_root,
    )


def local(query_rows, key_rows, value_rows, out_grad, log_totals, out_dot, bias_table):
    row_count = query_rows.shape[0]
    feature_count = query_rows.shape[1]
    head_count = log_totals.shape[1]
    seg_count = row_count // SEG_LEN
    span_segs = LEFT_SEGS + 1
    band_len = span_segs * SEG_LEN
    need_rows = LEFT_SEGS * SEG_LEN
    lag_total = -(-need_rows // row_count)
    skip_rows = lag_total * row_count - need_rows
    first_row = lax.axis_index(("sp", "tp")) * row_count
    earlier = []
    for lag_count in range(lag_total, 0, -1):
        start_row = skip_rows if lag_count == lag_total else 0
        earlier.append(passed_along((key_rows, value_rows), ("sp", "tp"), lag_count))
    all_keys = jnp.concatenate([pair[0] for pair in earlier] + [key_rows], axis=0)
    all_values = jnp.concatenate([pair[1] for pair in earlier] + [value_rows], axis=0)
    key_bands = band_stack(all_keys, seg_count, span_segs)
    value_bands = band_stack(all_values, seg_count, span_segs)
    band_pos = (
        jnp.arange(seg_count, dtype=jnp.int32)[:, None] * SEG_LEN
        + jnp.arange(band_len, dtype=jnp.int32)[None, :]
    )
    allowed = first_row - need_rows + band_pos >= 0
    bias_vals, onehot_map = bias_block(bias_table, need_rows, SEG_LEN, band_len)
    weights_b, score_grads_b, score_grads, query_heads, key_heads, grad_heads, inv_root = (
        band_terms(
            query_rows.reshape(seg_count, SEG_LEN, feature_count),
            out_grad.reshape(seg_count, SEG_LEN, feature_count),
            log_totals.reshape(seg_count, SEG_LEN, head_count),
            out_dot.reshape(seg_count, SEG_LEN, head_count),
            key_bands,
            value_bands,
            bias_vals,
            allowed,
        )
    )
    tap_part = jnp.dot(
        diagonal_sums(jnp.sum(score_grads, axis=0)), onehot_map, precision=lax.Precision.HIGHEST
    )
    query_part = jnp.einsum(
        "bhqk,bkhd->bqhd", score_grads_b, key_heads, preferred_element_type=jnp.float32
    )
    grad_query = (query_part * inv_root).reshape(row_count, feature_count).astype(jnp.bfloat16)
    key_band_grad = jnp.einsum(
        "bhqk,bqhd->bkhd", score_grads_b, query_heads, preferred_element_type=jnp.float32
    )
    key_band_grad = (key_band_grad * inv_root).reshape(seg_count, span_segs, SEG_LEN, feature_count)
    value_band_grad = jnp.einsum(
        "bhqk,bqhd->bkhd", weights_b, grad_heads, preferred_element_type=jnp.float32
    )
    value_band_grad = value_band_grad.reshape(seg_count, span_segs, SEG_LEN, feature_count)
    key_all = sum(
        (
            jnp.pad(key_band_grad[:, lag], ((lag, LEFT_SEGS - lag), (0, 0), (0, 0)))
            for lag in range(span_segs)
        )
    ).reshape(-1, feature_count)
    value_all = sum(
        (
            jnp.pad(value_band_grad[:, lag], ((lag, LEFT_SEGS - lag), (0, 0), (0, 0)))
            for lag in range(span_segs)
        )
    ).reshape(-1, feature_count)
    key_total = key_all[need_rows:]
    value_total = value_all[need_rows:]
    for lag_count in range(1, lag_total + 1):
        lower_row = max(need_rows - lag_count * row_count, 0)
        upper_row = need_rows - (lag_count - 1) * row_count
        returned = passed_along(
            (key_all[lower_row:upper_row], value_all[lower_row:upper_row]), ("sp", "tp"), -lag_count
        )
        lead_rows = row_count - (upper_row - lower_row)
        key_total = key_total + returned[0]
        value_total = value_total + returned[1]
    grad_table = lax.psum(tap_part, ("sp", "tp"))
    return (
        grad_query,
        key_total.astype(jnp.bfloat16),
        value_total.astype(jnp.bfloat16),
        grad_table,
    )


def solution(mesh):
    placed = (
        P(("sp", "tp"), None),
        P(("sp", "tp"), None),
        P(("sp", "tp"), None),
        P(("sp", "tp"), None),
        P(("sp", "tp"), None),
        P(("sp", "tp"), None),
        P(),
    )
    return jax.shard_map(
        local,
        mesh=mesh,
        in_specs=placed,
        out_specs=(P(("sp", "tp"), None), P(("sp", "tp"), None), P(("sp", "tp"), None), P()),
        check_vma=False,
    )
```

profile of v0, /device:TPU:0, one launch (start us, length us, event | category | flops | bytes accessed | tf_op | source)
XLA Modules:
  0.0 198.3 jit_solution(5561602564015735739)
XLA Ops:
  0.6 5.7 %collective-permute-start.1 = (bf16[256,1024]{1,0:T(8,128)(2,1)}, bf16[256,1024]{1,0:T(8,128)(2,1)}, u32[]{:S(2)}, u32[]{:S(2)}) collective-permute-start(bf16[256,1024]{1,0:T(8,128)(2,1)} %param.8), channel_id=1, source_target_pairs={{0,1},{1,2},{2,3},{3,4},{4,5},{5,6},{6,7},{7,8},{8,9},{9,10},{10,1... | collective-permute-start | bytes 1572872 | tf_op jit(solution)/shard_map/ppermute | solution.py:14
  6.3 2.1 %collective-permute-start = (bf16[256,1024]{1,0:T(8,128)(2,1)}, bf16[256,1024]{1,0:T(8,128)(2,1)}, u32[]{:S(2)}, u32[]{:S(2)}) collective-permute-start(bf16[256,1024]{1,0:T(8,128)(2,1)} %param.8), channel_id=1, source_target_pairs={{0,2},{1,3},{2,4},{3,5},{4,6},{5,7},{6,8},{7,9},{8,10},{9,11},{10,... | collective-permute-start | bytes 1572872 | tf_op jit(solution)/shard_map/ppermute | solution.py:14
  8.4 4.1 %collective-permute-start.3 = (bf16[256,1024]{1,0:T(8,128)(2,1)}, bf16[256,1024]{1,0:T(8,128)(2,1)}, u32[]{:S(2)}, u32[]{:S(2)}) collective-permute-start(bf16[256,1024]{1,0:T(8,128)(2,1)} %param.9), channel_id=1, source_target_pairs={{0,1},{1,2},{2,3},{3,4},{4,5},{5,6},{6,7},{7,8},{8,9},{9,10},{10,1... | collective-permute-start | bytes 1572872 | tf_op jit(solution)/shard_map/ppermute | solution.py:14
  12.6 2.1 %collective-permute-start.2 = (bf16[256,1024]{1,0:T(8,128)(2,1)}, bf16[256,1024]{1,0:T(8,128)(2,1)}, u32[]{:S(2)}, u32[]{:S(2)}) collective-permute-start(bf16[256,1024]{1,0:T(8,128)(2,1)} %param.9), channel_id=1, source_target_pairs={{0,2},{1,3},{2,4},{3,5},{4,6},{5,7},{6,8},{7,9},{8,10},{9,11},{10,... | collective-permute-start | bytes 1572872 | tf_op jit(solution)/shard_map/ppermute | solution.py:14
  14.7 0.6 convolution_bitcast_fusion.1
  15.4 0.8 reshape.116
  16.2 0.8 reshape.117
  16.9 1.1 copy.172
  18.1 1.9 copy.175
  20.1 0.7 reshape.114
  21.2 0.8 reverse
  22.4 1.1 constant_dynamic-update-slice_fusion.14
  23.5 1.1 constant_dynamic-update-slice_fusion.1
  24.6 3.6 %collective-permute-done.3 = bf16[256,1024]{1,0:T(8,128)(2,1)} collective-permute-done((bf16[256,1024]{1,0:T(8,128)(2,1)}, bf16[256,1024]{1,0:T(8,128)(2,1)}, u32[]{:S(2)}, u32[]{:S(2)}) %collective-permute-start.3) | collective-permute-done | bytes 524320 | tf_op jit(solution)/shard_map/ppermute | solution.py:14
  28.2 1.2 constant_dynamic-update-slice_fusion.16
  30.0 1.2 constant_dynamic-update-slice_fusion.3
  31.6 1.1 constant_dynamic-update-slice_fusion.25
  32.9 1.1 constant_dynamic-update-slice_fusion.21
  34.1 1.2 copy.174
  35.3 1.1 constant_dynamic-update-slice_fusion.12
  36.6 1.1 constant_dynamic-update-slice_fusion.8
  37.8 1.2 copy.171
  39.1 1.7 fusion.5
  41.3 5.0 %convolution_bitcast_fusion = f32[4,576,8,128]{3,1,2,0:T(8,128)} fusion(f32[4,8,576,64]{2,3,1,0:T(8,128)S(1)} %fusion.5, f32[4,8,64]{2,1,0:T(8,128)S(1)} %get-tuple-element.49, f32[8,64,576]{2,1,0:T(8,128)S(1)} %slice.268, pred[4,576]{1,0:T(4,128)(4,1)S(1)} %add_compare_fusion, bf16[4,64,8,128]{3,2,1,0:T(8,128)(2,1)S(1)} %bitcast.221), kind=kOutput, calls=%fused_computation.13 | convolution fusion | flops 307888128 | bytes 15870208 | tf_op jit(solution)/shard_map/bhqk,bqhd->bkhd/dot_general | solution.py:138
  46.3 4.2 %fusion.52 = (f32[8,64,576]{2,1,0:T(8,128)S(1)}, bf16[4,8,64,576]{3,2,1,0:T(8,128)(2,1)}) fusion(f32[4,8,64]{2,1,0:T(8,128)S(1)} %get-tuple-element.48, bf16[4,64,8,128]{3,2,1,0:T(8,128)(2,1)S(1)} %bitcast.222, bf16[4,576,8,128]{3,2,1,0:T(8,128)(2,1)S(1)} %bitcast.220, f32[4,8,64]{2,1,0:T(8,128)S(1)} %get-tuple-element.49, f32[8,64,576]{2,1,0:T(8,128)S(1)} %slice.268, ...), kind=kOutput, calls=%fused_computation.101 | convolution fusion | flops 311132160 | bytes 14698752 | tf_op jit(solution)/shard_map/bqhd,bkhd->bhqk/dot_general | solution.py:75
  50.5 1.0 reverse.1
  52.0 0.8 copy.177
  52.8 1.3 reshape.121
  54.2 12.8 %copy.146 = f32[4,576,8,128]{3,2,1,0:T(8,128)} copy(f32[4,576,8,128]{3,1,2,0:T(8,128)} %convolution_bitcast_fusion) | data formatting | bytes 18874368 | tf_op jit(solution)/shard_map/bhqk,bqhd->bkhd/transpose | solution.py:138
  67.0 11.2 %reshape.119 = f32[4,9,64,1024]{3,2,1,0:T(8,128)} reshape(f32[4,576,8,128]{3,2,1,0:T(8,128)} %copy.146) | data formatting | bytes 18874368 | tf_op jit(solution)/shard_map/reshape | solution.py:141
  78.2 4.7 %slice_bitcast_fusion.8 = (f32[4,64,1024]{2,1,0:T(8,128)S(1)}, f32[4,64,1024]{2,1,0:T(8,128)S(1)}, f32[4,64,1024]{2,1,0:T(8,128)S(1)}, f32[4,64,1024]{2,1,0:T(8,...) fusion(f32[4,9,64,1024]{3,2,1,0:T(8,128)} %reshape.119), kind=kLoop, calls=%fused_computation.37 | loop fusion | bytes 18874368 | tf_op jit(solution)/shard_map/squeeze | solution.py:150
  82.8 1.0 pad_add_fusion
  83.8 1.6 fusion.46
  85.5 1.3 collective-permute-start.7
  86.8 1.5 collective-permute-start.6
  88.3 1.5 multiply_bitcast_fusion
  89.8 9.1 %copy.136 = f32[4,576,8,128]{3,2,1,0:T(8,128)} copy(f32[4,576,8,128]{3,1,2,0:T(8,128)S(1)} %multiply_bitcast_fusion) | data formatting | bytes 18874368 | tf_op jit(solution)/shard_map/mul | solution.py:137
  98.9 11.1 %reshape.118 = f32[4,9,64,1024]{3,2,1,0:T(8,128)} reshape(f32[4,576,8,128]{3,2,1,0:T(8,128)} %copy.136) | data formatting | bytes 18874368 | tf_op jit(solution)/shard_map/reshape | solution.py:137
  110.0 4.7 %slice_bitcast_fusion.17 = (f32[4,64,1024]{2,1,0:T(8,128)S(1)}, f32[4,64,1024]{2,1,0:T(8,128)S(1)}, f32[4,64,1024]{2,1,0:T(8,128)S(1)}, f32[4,64,1024]{2,1,0:T(8...) fusion(f32[4,9,64,1024]{3,2,1,0:T(8,128)} %reshape.118), kind=kLoop, calls=%fused_computation.46 | loop fusion | bytes 18874368 | tf_op jit(solution)/shard_map/squeeze | solution.py:144
  114.8 1.0 pad_add_fusion.1
  115.8 1.7 fusion.47
  117.5 1.4 collective-permute-start.5
  118.9 1.3 collective-permute-start.4
  120.2 1.2 fusion.28
  121.8 0.9 copy.209
  123.2 70.2 %psum.7 = f32[8,320]{1,0:T(8,128)} all-reduce(f32[8,320]{1,0:T(8,128)S(1)} %fusion.37), channel_id=1, replica_groups=mesh['sp'=16,'tp'=2] {'sp','tp'}, use_global_device_ids=true, to_apply=%region_2.3 | all-reduce | flops 2560 | bytes 20480 | tf_op jit(solution)/shard_map/psum | solution.py:165
  193.4 2.6 %fusion.34 = bf16[256,1024]{1,0:T(8,128)(2,1)} fusion(f32[256,1024]{1,0:T(8,128)} %collective-permute-done.7, f32[256,1024]{1,0:T(8,128)} %collective-permute-done.6, f32[4,64,1024]{2,1,0:T(8,128)S(1)} %get-tuple-element.22), kind=kLoop, calls=%fused_computation.49 | loop fusion | flops 786432 | bytes 3670016 | tf_op jit(solution)/shard_map/convert_element_type | solution.py:169
  196.0 2.3 %fusion.36 = bf16[256,1024]{1,0:T(8,128)(2,1)} fusion(f32[256,1024]{1,0:T(8,128)S(1)} %collective-permute-done.5, f32[256,1024]{1,0:T(8,128)} %collective-permute-done.4, f32[4,64,1024]{2,1,0:T(8,128)S(1)} %get-tuple-element.25), kind=kLoop, calls=%fused_computation.52 | loop fusion | flops 786432 | bytes 3670016 | tf_op jit(solution)/shard_map/convert_element_type | solution.py:168
  (59 shorter events, 4.3 us)
Async XLA Ops:
  0.6 14.0 %copy-start = (f32[8,320]{1,0:T(8,128)S(1)}, f32[8,320]{1,0:T(8,128)}, u32[]{:S(2)}) copy-start(f32[8,320]{1,0:T(8,128)} %param.13) | copy-start | bytes 30724
  0.6 29.3 %collective-permute-start.1 = (bf16[256,1024]{1,0:T(8,128)(2,1)}, bf16[256,1024]{1,0:T(8,128)(2,1)}, u32[]{:S(2)}, u32[]{:S(2)}) collective-permute-start(bf16[256,1024]{1,0:T(8,128)(2,1)} %param.8), channel_id=1, source_target_pairs={{0,1},{1,2},{2,3},{3,4},{4,5},{5,6},{6,7},{7,8},{8,9},{9,10},{10,1... | collective-permute-start | bytes 1572872 | tf_op jit(solution)/shard_map/ppermute | solution.py:14
  6.3 17.2 %collective-permute-start = (bf16[256,1024]{1,0:T(8,128)(2,1)}, bf16[256,1024]{1,0:T(8,128)(2,1)}, u32[]{:S(2)}, u32[]{:S(2)}) collective-permute-start(bf16[256,1024]{1,0:T(8,128)(2,1)} %param.8), channel_id=1, source_target_pairs={{0,2},{1,3},{2,4},{3,5},{4,6},{5,7},{6,8},{7,9},{8,10},{9,11},{10,... | collective-permute-start | bytes 1572872 | tf_op jit(solution)/shard_map/ppermute | solution.py:14
  8.4 19.8 %collective-permute-start.3 = (bf16[256,1024]{1,0:T(8,128)(2,1)}, bf16[256,1024]{1,0:T(8,128)(2,1)}, u32[]{:S(2)}, u32[]{:S(2)}) collective-permute-start(bf16[256,1024]{1,0:T(8,128)(2,1)} %param.9), channel_id=1, source_target_pairs={{0,1},{1,2},{2,3},{3,4},{4,5},{5,6},{6,7},{7,8},{8,9},{9,10},{10,1... | collective-permute-start | bytes 1572872 | tf_op jit(solution)/shard_map/ppermute | solution.py:14
  12.6 9.9 %collective-permute-start.2 = (bf16[256,1024]{1,0:T(8,128)(2,1)}, bf16[256,1024]{1,0:T(8,128)(2,1)}, u32[]{:S(2)}, u32[]{:S(2)}) collective-permute-start(bf16[256,1024]{1,0:T(8,128)(2,1)} %param.9), channel_id=1, source_target_pairs={{0,2},{1,3},{2,4},{3,5},{4,6},{5,7},{6,8},{7,9},{8,10},{9,11},{10,... | collective-permute-start | bytes 1572872 | tf_op jit(solution)/shard_map/ppermute | solution.py:14
  22.0 7.4 %copy-start.6 = (bf16[256,1024]{1,0:T(8,128)(2,1)S(1)}, bf16[256,1024]{1,0:T(8,128)(2,1)}, u32[]{:S(2)}) copy-start(bf16[256,1024]{1,0:T(8,128)(2,1)} %param.9) | copy-start | bytes 1572868
  29.4 1.7 copy-start.7
  39.0 2.2 %copy-start.2 = (bf16[288,8,8,128]{3,2,1,0:T(8,128)(2,1)}, bf16[288,8,8,128]{3,2,1,0:T(8,128)(2,1)S(1)}, u32[]{:S(2)}) copy-start(bf16[288,8,8,128]{3,2,1,0:T(8,128)(2,1)S(1)} %copy.171) | copy-start | bytes 14155780
  39.1 2.2 %copy-start.5 = (bf16[32,8,8,128]{3,2,1,0:T(8,128)(2,1)S(1)}, bf16[32,8,8,128]{3,2,1,0:T(8,128)(2,1)}, u32[]{:S(2)}) copy-start(bf16[32,8,8,128]{3,2,1,0:T(8,128)(2,1)} %copy.175) | copy-start | bytes 1572868
  83.8 4.5 %copy-start.3 = (bf16[4,8,64,576]{3,2,1,0:T(8,128)(2,1)S(1)}, bf16[4,8,64,576]{3,2,1,0:T(8,128)(2,1)}, u32[]{:S(2)}) copy-start(bf16[4,8,64,576]{3,2,1,0:T(8,128)(2,1)} %get-tuple-element.45) | copy-start | bytes 7077892
  85.5 107.9 %collective-permute-start.7 = (f32[256,1024]{1,0:T(8,128)}, f32[256,1024]{1,0:T(8,128)}, u32[]{:S(2)}, u32[]{:S(2)}) collective-permute-start(f32[256,1024]{1,0:T(8,128)} %bitcast.67), channel_id=1, source_target_pairs={{2,0},{3,1},{4,2},{5,3},{6,4},{7,5},{8,6},{9,7},{10,8},{11,9},{12,... | collective-permute-start | bytes 3145736 | tf_op jit(solution)/shard_map/ppermute | solution.py:14
  86.8 106.6 %collective-permute-start.6 = (f32[256,1024]{1,0:T(8,128)}, f32[256,1024]{1,0:T(8,128)}, u32[]{:S(2)}, u32[]{:S(2)}) collective-permute-start(f32[256,1024]{1,0:T(8,128)} %bitcast.66), channel_id=1, source_target_pairs={{1,0},{2,1},{3,2},{4,3},{5,4},{6,5},{7,6},{8,7},{9,8},{10,9},{11,1... | collective-permute-start | bytes 3145736 | tf_op jit(solution)/shard_map/ppermute | solution.py:14
  110.0 10.2 %slice-start = ((s8[4718592]{0:T(1024)(128)(4,1)}), s8[524288]{0:T(1024)(128)(4,1)S(1)}, s32[]{:S(2)}) async-start(s8[4718592]{0:T(1024)(128)(4,1)} %bitcast.210), calls=%async_computation | async-start | bytes 1048576
  114.8 5.4 %slice-start.1 = ((s8[4718592]{0:T(1024)(128)(4,1)}), s8[4194304]{0:T(1024)(128)(4,1)S(1)}, s32[]{:S(2)}) async-start(s8[4718592]{0:T(1024)(128)(4,1)} %bitcast.210), calls=%async_computation.1 | async-start | bytes 8388608
  115.8 4.4 %copy-start.4 = (bf16[4,8,64,576]{3,2,1,0:T(8,128)(2,1)S(1)}, bf16[4,8,64,576]{3,2,1,0:T(8,128)(2,1)}, u32[]{:S(2)}) copy-start(bf16[4,8,64,576]{3,2,1,0:T(8,128)(2,1)} %get-tuple-element.45) | copy-start | bytes 7077892
  117.5 78.5 %collective-permute-start.5 = (f32[256,1024]{1,0:T(8,128)}, f32[256,1024]{1,0:T(8,128)S(1)}, u32[]{:S(2)}, u32[]{:S(2)}) collective-permute-start(f32[256,1024]{1,0:T(8,128)} %bitcast.54), channel_id=1, source_target_pairs={{2,0},{3,1},{4,2},{5,3},{6,4},{7,5},{8,6},{9,7},{10,8},{11,9},{12,... | collective-permute-start | bytes 3145736 | tf_op jit(solution)/shard_map/ppermute | solution.py:14
  118.9 77.1 %collective-permute-start.4 = (f32[256,1024]{1,0:T(8,128)}, f32[256,1024]{1,0:T(8,128)}, u32[]{:S(2)}, u32[]{:S(2)}) collective-permute-start(f32[256,1024]{1,0:T(8,128)} %bitcast.53), channel_id=1, source_target_pairs={{1,0},{2,1},{3,2},{4,3},{5,4},{6,5},{7,6},{8,7},{9,8},{10,9},{11,1... | collective-permute-start | bytes 3145736 | tf_op jit(solution)/shard_map/ppermute | solution.py:14
  120.2 78.0 %copy-start.1 = (f32[8,320]{1,0:T(8,128)S(1)}, f32[8,320]{1,0:T(8,128)}, u32[]{:S(2)}) copy-start(f32[8,320]{1,0:T(8,128)} %param.13) | copy-start | bytes 30724
where the time goes:
time: 200 us; the launch traced here: 198 us
  local copies, waits for them, and re-layouts  81.9 us (41%)
  blocking collectives  70.2 us (35%)
  starting transfers between devices  19.5 us (10%)
  matrix products  14.8 us (7%)
  other arithmetic  7.04 us (4%)
  waiting for transfers between devices  3.66 us (2%)
    psum x1, blocking collectives, local(): grad_table = lax.psum(tap_part, ('sp', 'tp'))  70.2 us
    unnamed x52, local copies, waits for them, and re-layouts  19.8 us
    ppermute x8, starting transfers between devices, passed_along(): return lax.ppermute(block, axis, route)  19.5 us
    transpose x1, local copies, waits for them, and re-layouts, local(): jnp.einsum('bhqk,bqhd->bkhd', weights_b, grad_heads, preferred_element_ty...  12.8 us
    reshape x1, local copies, waits for them, and re-layouts, local(): value_band_grad.reshape(seg_count, span_segs, SEG_LEN, feature_count)  11.2 us
    reshape x1, local copies, waits for them, and re-layouts, local(): (key_band_grad * inv_root).reshape(seg_count, span_segs, SEG_LEN, feature...  11.1 us
    mul x1, local copies, waits for them, and re-layouts, local(): key_band_grad * inv_root  9.13 us
    dot_general x1, matrix products, local(): jnp.einsum('bhqk,bqhd->bkhd', weights_b, grad_heads, preferred_element_ty...  5.01 us
  transfers between devices with their start and end apart: 8, of which 1 were waited for; matrix products, arithmetic and copies ran while one was open for 23% of the time, Pallas kernels for 0%

commit v1 on v0

--- a/solution.py
+++ b/solution.py
@@ -162,7 +162,7 @@
         lead_rows = row_count - (upper_row - lower_row)
         key_total = key_total + returned[0]
         value_total = value_total + returned[1]
-    grad_table = lax.psum(tap_part, ("sp", "tp"))
+    grad_table = lax.psum(lax.psum(tap_part, "tp"), "sp")
     return (
         grad_query,
         key_total.astype(jnp.bfloat16),

time: 200 us -> 228 us (1.14)
  blocking collectives: 70.2 us -> 98.6 us
    psum x1 -> x2, blocking collectives: 70.2 us -> 98.6 us  [local(): grad_table = lax.psum(lax.psum(tap_part, 'tp'), 'sp')]
  transfers between devices with their start and end apart: 8 -> 8, of which waited for: 1 -> 1; matrix products, arithmetic and copies ran while one was open for 23% -> 20% of each run, Pallas kernels for 0% -> 0%
where the time goes in v1:
time: 228 us; the launch traced here: 227 us
  blocking collectives  98.6 us (43%)
  local copies, waits for them, and re-layouts  82 us (36%)
  starting transfers between devices  19.5 us (9%)
  matrix products  14.8 us (6%)
  other arithmetic  7.03 us (3%)
  waiting for transfers between devices  3.63 us (2%)
    psum x2, blocking collectives, local(): grad_table = lax.psum(lax.psum(tap_part, 'tp'), 'sp')  98.6 us
    unnamed x52, local copies, waits for them, and re-layouts  19.8 us
    ppermute x8, starting transfers between devices, passed_along(): return lax.ppermute(block, axis, route)  19.5 us
    transpose x1, local copies, waits for them, and re-layouts, local(): jnp.einsum('bhqk,bqhd->bkhd', weights_b, grad_heads, preferred_element_ty...  12.8 us
    reshape x1, local copies, waits for them, and re-layouts, local(): value_band_grad.reshape(seg_count, span_segs, SEG_LEN, feature_count)  11.2 us
    reshape x1, local copies, waits for them, and re-layouts, local(): (key_band_grad * inv_root).reshape(seg_count, span_segs, SEG_LEN, feature...  11.1 us
    mul x1, local copies, waits for them, and re-layouts, local(): key_band_grad * inv_root  9.11 us
    dot_general x1, matrix products, local(): jnp.einsum('bhqk,bqhd->bkhd', weights_b, grad_heads, preferred_element_ty...  4.99 us
  transfers between devices with their start and end apart: 8, of which 1 were waited for; matrix products, arithmetic and copies ran while one was open for 20% of the time, Pallas kernels for 0%

profile of v1, /device:TPU:0, one launch (start us, length us, event | category | flops | bytes accessed | tf_op | source)
XLA Modules:
  0.0 226.7 jit_solution(13026739323105482837)
XLA Ops:
  0.6 5.7 %collective-permute-start.1 = (bf16[256,1024]{1,0:T(8,128)(2,1)}, bf16[256,1024]{1,0:T(8,128)(2,1)}, u32[]{:S(2)}, u32[]{:S(2)}) collective-permute-start(bf16[256,1024]{1,0:T(8,128)(2,1)} %param.8), channel_id=1, source_target_pairs={{0,1},{1,2},{2,3},{3,4},{4,5},{5,6},{6,7},{7,8},{8,9},{9,10},{10,1... | collective-permute-start | bytes 1572872 | tf_op jit(solution)/shard_map/ppermute | solution.py:14
  6.3 2.1 collective-permute-start
  8.4 4.2 %collective-permute-start.3 = (bf16[256,1024]{1,0:T(8,128)(2,1)}, bf16[256,1024]{1,0:T(8,128)(2,1)}, u32[]{:S(2)}, u32[]{:S(2)}) collective-permute-start(bf16[256,1024]{1,0:T(8,128)(2,1)} %param.9), channel_id=1, source_target_pairs={{0,1},{1,2},{2,3},{3,4},{4,5},{5,6},{6,7},{7,8},{8,9},{9,10},{10,1... | collective-permute-start | bytes 1572872 | tf_op jit(solution)/shard_map/ppermute | solution.py:14
  12.6 2.1 collective-permute-start.2
  15.4 0.8 reshape.116
  16.2 0.8 reshape.117
  17.0 1.1 copy.172
  18.1 1.9 copy.175
  20.1 0.7 reshape.114
  21.2 0.8 reverse
  22.5 1.1 constant_dynamic-update-slice_fusion.14
  23.6 1.1 constant_dynamic-update-slice_fusion.1
  24.6 3.6 %collective-permute-done.3 = bf16[256,1024]{1,0:T(8,128)(2,1)} collective-permute-done((bf16[256,1024]{1,0:T(8,128)(2,1)}, bf16[256,1024]{1,0:T(8,128)(2,1)}, u32[]{:S(2)}, u32[]{:S(2)}) %collective-permute-start.3) | collective-permute-done | bytes 524320 | tf_op jit(solution)/shard_map/ppermute | solution.py:14
  28.2 1.2 constant_dynamic-update-slice_fusion.16
  30.0 1.2 constant_dynamic-update-slice_fusion.3
  31.6 1.1 constant_dynamic-update-slice_fusion.25
  32.9 1.1 constant_dynamic-update-slice_fusion.21
  34.1 1.2 copy.174
  35.3 1.1 constant_dynamic-update-slice_fusion.12
  36.6 1.1 constant_dynamic-update-slice_fusion.8
  37.8 1.2 copy.171
  39.1 1.7 fusion.5
  41.3 5.0 %convolution_bitcast_fusion = f32[4,576,8,128]{3,1,2,0:T(8,128)} fusion(f32[4,8,576,64]{2,3,1,0:T(8,128)S(1)} %fusion.5, f32[4,8,64]{2,1,0:T(8,128)S(1)} %get-tuple-element.49, f32[8,64,576]{2,1,0:T(8,128)S(1)} %slice.268, pred[4,576]{1,0:T(4,128)(4,1)S(1)} %add_compare_fusion, bf16[4,64,8,128]{3,2,1,0:T(8,128)(2,1)S(1)} %bitcast.221), kind=kOutput, calls=%fused_computation.13 | convolution fusion | flops 307888128 | bytes 15870208 | tf_op jit(solution)/shard_map/bhqk,bqhd->bkhd/dot_general | solution.py:138
  46.2 4.3 %fusion.52 = (f32[8,64,576]{2,1,0:T(8,128)S(1)}, bf16[4,8,64,576]{3,2,1,0:T(8,128)(2,1)}) fusion(f32[4,8,64]{2,1,0:T(8,128)S(1)} %get-tuple-element.48, bf16[4,64,8,128]{3,2,1,0:T(8,128)(2,1)S(1)} %bitcast.222, bf16[4,576,8,128]{3,2,1,0:T(8,128)(2,1)S(1)} %bitcast.220, f32[4,8,64]{2,1,0:T(8,128)S(1)} %get-tuple-element.49, f32[8,64,576]{2,1,0:T(8,128)S(1)} %slice.268, ...), kind=kOutput, calls=%fused_computation.101 | convolution fusion | flops 311132160 | bytes 14698752 | tf_op jit(solution)/shard_map/bqhd,bkhd->bhqk/dot_general | solution.py:75
  50.5 1.0 reverse.1
  52.0 0.8 copy.177
  52.7 1.3 reshape.121
  54.2 12.8 %copy.146 = f32[4,576,8,128]{3,2,1,0:T(8,128)} copy(f32[4,576,8,128]{3,1,2,0:T(8,128)} %convolution_bitcast_fusion) | data formatting | bytes 18874368 | tf_op jit(solution)/shard_map/bhqk,bqhd->bkhd/transpose | solution.py:138
  67.0 11.2 %reshape.119 = f32[4,9,64,1024]{3,2,1,0:T(8,128)} reshape(f32[4,576,8,128]{3,2,1,0:T(8,128)} %copy.146) | data formatting | bytes 18874368 | tf_op jit(solution)/shard_map/reshape | solution.py:141
  78.2 4.7 %slice_bitcast_fusion.8 = (f32[4,64,1024]{2,1,0:T(8,128)S(1)}, f32[4,64,1024]{2,1,0:T(8,128)S(1)}, f32[4,64,1024]{2,1,0:T(8,128)S(1)}, f32[4,64,1024]{2,1,0:T(8,...) fusion(f32[4,9,64,1024]{3,2,1,0:T(8,128)} %reshape.119), kind=kLoop, calls=%fused_computation.37 | loop fusion | bytes 18874368 | tf_op jit(solution)/shard_map/squeeze | solution.py:150
  82.9 1.0 pad_add_fusion
  83.9 1.6 fusion.46
  85.5 1.3 collective-permute-start.7
  86.8 1.5 collective-permute-start.6
  88.3 1.5 multiply_bitcast_fusion
  89.8 9.1 %copy.136 = f32[4,576,8,128]{3,2,1,0:T(8,128)} copy(f32[4,576,8,128]{3,1,2,0:T(8,128)S(1)} %multiply_bitcast_fusion) | data formatting | bytes 18874368 | tf_op jit(solution)/shard_map/mul | solution.py:137
  98.9 11.1 %reshape.118 = f32[4,9,64,1024]{3,2,1,0:T(8,128)} reshape(f32[4,576,8,128]{3,2,1,0:T(8,128)} %copy.136) | data formatting | bytes 18874368 | tf_op jit(solution)/shard_map/reshape | solution.py:137
  110.0 4.7 %slice_bitcast_fusion.17 = (f32[4,64,1024]{2,1,0:T(8,128)S(1)}, f32[4,64,1024]{2,1,0:T(8,128)S(1)}, f32[4,64,1024]{2,1,0:T(8,128)S(1)}, f32[4,64,1024]{2,1,0:T(8...) fusion(f32[4,9,64,1024]{3,2,1,0:T(8,128)} %reshape.118), kind=kLoop, calls=%fused_computation.46 | loop fusion | bytes 18874368 | tf_op jit(solution)/shard_map/squeeze | solution.py:144
  114.8 1.0 pad_add_fusion.1
  115.8 1.7 fusion.47
  117.5 1.4 collective-permute-start.5
  118.9 1.3 collective-permute-start.4
  120.3 1.2 fusion.28
  121.8 0.9 copy.209
  123.2 21.6 %psum.14 = f32[8,320]{1,0:T(8,128)S(1)} all-reduce(f32[8,320]{1,0:T(8,128)S(1)} %fusion.37), channel_id=1, replica_groups=mesh['sp'=16,'tp'=2] {'tp'}, use_global_device_ids=true, to_apply=%region_2.3 | all-reduce | flops 2560 | bytes 20480 | tf_op jit(solution)/shard_map/psum | solution.py:165
  144.8 77.0 %psum.15 = f32[8,320]{1,0:T(8,128)} all-reduce(f32[8,320]{1,0:T(8,128)S(1)} %psum.14), channel_id=1, replica_groups=mesh['sp'=16,'tp'=2] {'sp'}, use_global_device_ids=true, to_apply=%region_3.4 | all-reduce | flops 2560 | bytes 20480 | tf_op jit(solution)/shard_map/psum | solution.py:165
  221.8 2.6 %fusion.34 = bf16[256,1024]{1,0:T(8,128)(2,1)} fusion(f32[256,1024]{1,0:T(8,128)} %collective-permute-done.7, f32[256,1024]{1,0:T(8,128)} %collective-permute-done.6, f32[4,64,1024]{2,1,0:T(8,128)S(1)} %get-tuple-element.22), kind=kLoop, calls=%fused_computation.49 | loop fusion | flops 786432 | bytes 3670016 | tf_op jit(solution)/shard_map/convert_element_type | solution.py:169
  224.4 2.3 %fusion.36 = bf16[256,1024]{1,0:T(8,128)(2,1)} fusion(f32[256,1024]{1,0:T(8,128)S(1)} %collective-permute-done.5, f32[256,1024]{1,0:T(8,128)} %collective-permute-done.4, f32[4,64,1024]{2,1,0:T(8,128)S(1)} %get-tuple-element.25), kind=kLoop, calls=%fused_computation.52 | loop fusion | flops 786432 | bytes 3670016 | tf_op jit(solution)/shard_map/convert_element_type | solution.py:168
  (60 shorter events, 4.9 us)
Async XLA Ops:
  0.6 14.1 %copy-start = (f32[8,320]{1,0:T(8,128)S(1)}, f32[8,320]{1,0:T(8,128)}, u32[]{:S(2)}) copy-start(f32[8,320]{1,0:T(8,128)} %param.13) | copy-start | bytes 30724
  0.6 29.3 %collective-permute-start.1 = (bf16[256,1024]{1,0:T(8,128)(2,1)}, bf16[256,1024]{1,0:T(8,128)(2,1)}, u32[]{:S(2)}, u32[]{:S(2)}) collective-permute-start(bf16[256,1024]{1,0:T(8,128)(2,1)} %param.8), channel_id=1, source_target_pairs={{0,1},{1,2},{2,3},{3,4},{4,5},{5,6},{6,7},{7,8},{8,9},{9,10},{10,1... | collective-permute-start | bytes 1572872 | tf_op jit(solution)/shard_map/ppermute | solution.py:14
  6.3 17.2 %collective-permute-start = (bf16[256,1024]{1,0:T(8,128)(2,1)}, bf16[256,1024]{1,0:T(8,128)(2,1)}, u32[]{:S(2)}, u32[]{:S(2)}) collective-permute-start(bf16[256,1024]{1,0:T(8,128)(2,1)} %param.8), channel_id=1, source_target_pairs={{0,2},{1,3},{2,4},{3,5},{4,6},{5,7},{6,8},{7,9},{8,10},{9,11},{10,... | collective-permute-start | bytes 1572872 | tf_op jit(solution)/shard_map/ppermute | solution.py:14
  8.4 19.8 %collective-permute-start.3 = (bf16[256,1024]{1,0:T(8,128)(2,1)}, bf16[256,1024]{1,0:T(8,128)(2,1)}, u32[]{:S(2)}, u32[]{:S(2)}) collective-permute-start(bf16[256,1024]{1,0:T(8,128)(2,1)} %param.9), channel_id=1, source_target_pairs={{0,1},{1,2},{2,3},{3,4},{4,5},{5,6},{6,7},{7,8},{8,9},{9,10},{10,1... | collective-permute-start | bytes 1572872 | tf_op jit(solution)/shard_map/ppermute | solution.py:14
  12.6 9.9 %collective-permute-start.2 = (bf16[256,1024]{1,0:T(8,128)(2,1)}, bf16[256,1024]{1,0:T(8,128)(2,1)}, u32[]{:S(2)}, u32[]{:S(2)}) collective-permute-start(bf16[256,1024]{1,0:T(8,128)(2,1)} %param.9), channel_id=1, source_target_pairs={{0,2},{1,3},{2,4},{3,5},{4,6},{5,7},{6,8},{7,9},{8,10},{9,11},{10,... | collective-permute-start | bytes 1572872 | tf_op jit(solution)/shard_map/ppermute | solution.py:14
  22.0 7.4 %copy-start.6 = (bf16[256,1024]{1,0:T(8,128)(2,1)S(1)}, bf16[256,1024]{1,0:T(8,128)(2,1)}, u32[]{:S(2)}) copy-start(bf16[256,1024]{1,0:T(8,128)(2,1)} %param.9) | copy-start | bytes 1572868
  29.4 1.7 copy-start.7
  39.0 2.2 copy-start.2
  39.1 2.2 copy-start.5
  83.9 4.5 %copy-start.3 = (bf16[4,8,64,576]{3,2,1,0:T(8,128)(2,1)S(1)}, bf16[4,8,64,576]{3,2,1,0:T(8,128)(2,1)}, u32[]{:S(2)}) copy-start(bf16[4,8,64,576]{3,2,1,0:T(8,128)(2,1)} %get-tuple-element.45) | copy-start | bytes 7077892
  85.5 136.3 %collective-permute-start.7 = (f32[256,1024]{1,0:T(8,128)}, f32[256,1024]{1,0:T(8,128)}, u32[]{:S(2)}, u32[]{:S(2)}) collective-permute-start(f32[256,1024]{1,0:T(8,128)} %bitcast.67), channel_id=1, source_target_pairs={{2,0},{3,1},{4,2},{5,3},{6,4},{7,5},{8,6},{9,7},{10,8},{11,9},{12,... | collective-permute-start | bytes 3145736 | tf_op jit(solution)/shard_map/ppermute | solution.py:14
  86.8 135.0 %collective-permute-start.6 = (f32[256,1024]{1,0:T(8,128)}, f32[256,1024]{1,0:T(8,128)}, u32[]{:S(2)}, u32[]{:S(2)}) collective-permute-start(f32[256,1024]{1,0:T(8,128)} %bitcast.66), channel_id=1, source_target_pairs={{1,0},{2,1},{3,2},{4,3},{5,4},{6,5},{7,6},{8,7},{9,8},{10,9},{11,1... | collective-permute-start | bytes 3145736 | tf_op jit(solution)/shard_map/ppermute | solution.py:14
  110.0 10.2 %slice-start = ((s8[4718592]{0:T(1024)(128)(4,1)}), s8[524288]{0:T(1024)(128)(4,1)S(1)}, s32[]{:S(2)}) async-start(s8[4718592]{0:T(1024)(128)(4,1)} %bitcast.210), calls=%async_computation | async-start | bytes 1048576
  114.8 5.4 %slice-start.1 = ((s8[4718592]{0:T(1024)(128)(4,1)}), s8[4194304]{0:T(1024)(128)(4,1)S(1)}, s32[]{:S(2)}) async-start(s8[4718592]{0:T(1024)(128)(4,1)} %bitcast.210), calls=%async_computation.1 | async-start | bytes 8388608
  115.8 4.4 %copy-start.4 = (bf16[4,8,64,576]{3,2,1,0:T(8,128)(2,1)S(1)}, bf16[4,8,64,576]{3,2,1,0:T(8,128)(2,1)}, u32[]{:S(2)}) copy-start(bf16[4,8,64,576]{3,2,1,0:T(8,128)(2,1)} %get-tuple-element.45) | copy-start | bytes 7077892
  117.5 106.9 %collective-permute-start.5 = (f32[256,1024]{1,0:T(8,128)}, f32[256,1024]{1,0:T(8,128)S(1)}, u32[]{:S(2)}, u32[]{:S(2)}) collective-permute-start(f32[256,1024]{1,0:T(8,128)} %bitcast.54), channel_id=1, source_target_pairs={{2,0},{3,1},{4,2},{5,3},{6,4},{7,5},{8,6},{9,7},{10,8},{11,9},{12,... | collective-permute-start | bytes 3145736 | tf_op jit(solution)/shard_map/ppermute | solution.py:14
  118.9 105.5 %collective-permute-start.4 = (f32[256,1024]{1,0:T(8,128)}, f32[256,1024]{1,0:T(8,128)}, u32[]{:S(2)}, u32[]{:S(2)}) collective-permute-start(f32[256,1024]{1,0:T(8,128)} %bitcast.53), channel_id=1, source_target_pairs={{1,0},{2,1},{3,2},{4,3},{5,4},{6,5},{7,6},{8,7},{9,8},{10,9},{11,1... | collective-permute-start | bytes 3145736 | tf_op jit(solution)/shard_map/ppermute | solution.py:14
  120.2 106.5 %copy-start.1 = (f32[8,320]{1,0:T(8,128)S(1)}, f32[8,320]{1,0:T(8,128)}, u32[]{:S(2)}) copy-start(f32[8,320]{1,0:T(8,128)} %param.13) | copy-start | bytes 30724
